TPU v7x, 32 devices: a whole 2x2x4 slice. The times are simulated.
32 devices in a mesh: sp: 8 (over z, core), tp: 4 (over y, x).
Axes of the slice: x: 2, y: 2, z: 4, core: 2. Of those that a mesh axis runs over, the one named last changes fastest.
Arguments:
- residual_in: bfloat16 [2048, 2048], P(('sp', 'tp')), may hold values from -6 to 6
- query_a: bfloat16 [2048, 1024], P('sp', 'tp'), may hold values from -12 to 12
- key_a: bfloat16 [2048, 1024], P('sp', 'tp'), may hold values from -12 to 12
- value_a: bfloat16 [2048, 1024], P('sp', 'tp'), may hold values from -6 to 6
- query_b: bfloat16 [2048, 2048], P('sp', 'tp'), may hold values from -12 to 12
- key_b: bfloat16 [2048, 2048], P('sp', 'tp'), may hold values from -12 to 12
- value_b: bfloat16 [2048, 2048], P('sp', 'tp'), may hold values from -6 to 6
- cum_gates: float32 [2048, 2, 16], P('sp', None, 'tp'), may hold values from -247.76 to 0, as said below
- out_a: bfloat16 [1024, 2048], P('tp'), may hold values from -0.1875 to 0.1875
- out_b: bfloat16 [2048, 2048], P('tp'), may hold values from -0.125 to 0.125
- post_gain: bfloat16 [2048], replicated, may hold values from 0.099609375 to 1.8984375
- pre_gain: bfloat16 [2048], replicated, may hold values from 0.099609375 to 1.8984375
- expert_ids: int32 [2048, 2], P('sp'), may hold values from 0 to 7, all different within a row; in each aligned block of 256 rows (0 to 255, 256 to 511, ...) at most 80 rows name the same one
- expert_weights: float32 [2048, 2], P('sp'), may hold values from 0.2 to 1
- w_gate: bfloat16 [8, 2048, 4096], P('sp', None, 'tp'), may hold values from -0.125 to 0.125
- w_up: bfloat16 [8, 2048, 4096], P('sp', None, 'tp'), may hold values from -0.125 to 0.125
- w_down: bfloat16 [8, 4096, 2048], P('sp', 'tp'), may hold values from -0.09375 to 0.09375
Outputs:
- layer_out: bfloat16 [2048, 2048], P(('sp', 'tp'))
Inputs may be any that keep to these rules, and one draw needn't show every extreme that they name: `expert_ids`: in each aligned block of 256 positions no expert is named by more than 80 routes, a bound that some block reaches; a token's experts differ. `cum_gates`: never rises along the positions.
All inputs are finite; a program needn't handle non-finite values.
Results may differ from a plain program's by a relative error of at most 0.015.
Values may be sent and summed in bfloat16 or wider, within the bound.
A program may use at most 64 MiB of HBM per device.

v0:
```python
import jax
import jax.numpy as jnp
from jax import lax
from jax.sharding import PartitionSpec as P

eps_norm = 1e-06
big_neg = -1e30


def rms_scale(values, gain):
    return values * lax.rsqrt(jnp.mean(values * values, axis=-1, keepdims=True) + eps_norm) * gain


def empty_state(item_count, heads, width):
    return (
        jnp.full((heads, item_count), big_neg, jnp.float32),
        jnp.zeros((heads, item_count), jnp.float32),
        jnp.zeros((heads, item_count, width), jnp.float32),
    )


def update_state(state, query, key_rows, values, query_gate, key_gate, mask, width):
    highest, total, accum = state
    score = jnp.einsum(
        "rhd,khd->hrk", query, key_rows, preferred_element_type=jnp.float32
    ) * width ** (-0.5)
    score = score + query_gate.T[:, :, None] - key_gate.T[:, None, :]
    new_high = jnp.maximum(highest, jnp.max(jnp.where(mask[None], score, big_neg), axis=2))
    expo = jnp.exp(jnp.where(mask[None], score - new_high[:, :, None], big_neg))
    total = jnp.sum(expo, axis=2)
    accum = jnp.einsum(
        "hrk,khd->hrd", expo.astype(jnp.bfloat16), values, preferred_element_type=jnp.float32
    )
    return (new_high, total, accum)


def finish(state):
    highest, total, accum = state
    heads, item_count, width = accum.shape
    result = accum / total[:, :, None]
    return result.transpose(1, 0, 2).reshape(item_count, heads * width).astype(jnp.bfloat16)


def per_device(
    residual_in,
    query_a,
    key_a,
    value_a,
    query_b,
    key_b,
    value_b,
    cum_gates,
    out_a,
    out_b,
    post_gain,
    pre_gain,
    expert_ids,
    expert_weights,
    w_gate,
    w_up,
    w_down,
):
    rows = query_a.shape[0]
    heads = cum_gates.shape[2]
    width_a = query_a.shape[1] // heads
    width_b = query_b.shape[1] // heads
    group_size = lax.axis_size("sp")
    narrow = lax.axis_size("tp")
    here = lax.axis_index("sp")
    offset = here * rows
    gates_all = lax.all_gather(cum_gates, "sp", axis=0, tiled=True)
    queries_a = query_a.reshape(rows, heads, width_a)
    queries_b = query_b.reshape(rows, heads, width_b)
    blocks = [(queries_a, queries_b, offset + jnp.arange(rows, dtype=jnp.int32), cum_gates)]
    initial = tuple(
        (
            (
                empty_state(block[2].shape[0], heads, width_a),
                empty_state(block[2].shape[0], heads, width_b),
            )
            for block in blocks
        )
    )
    start = jnp.int32(0)
    piece_key_a = lax.all_gather(key_a.reshape(rows, heads, width_a), "sp", axis=0, tiled=True)
    piece_value_a = lax.all_gather(value_a.reshape(rows, heads, width_a), "sp", axis=0, tiled=True)
    piece_key_b = lax.all_gather(key_b.reshape(rows, heads, width_b), "sp", axis=0, tiled=True)
    piece_value_b = lax.all_gather(value_b.reshape(rows, heads, width_b), "sp", axis=0, tiled=True)
    item_count = piece_key_a.shape[0]
    key_pos = jnp.arange(item_count, dtype=jnp.int32)
    updated = []
    for state, (block_a, block_b, position, block_gate) in zip(initial, blocks):

        def compute(current):
            mask = key_pos[None, :] <= position[:, None]
            return (
                update_state(
                    current[0],
                    block_a,
                    piece_key_a,
                    piece_value_a,
                    block_gate[:, 0, :],
                    gates_all[:, 0, :],
                    mask,
                    width_a,
                ),
                update_state(
                    current[1],
                    block_b,
                    piece_key_b,
                    piece_value_b,
                    block_gate[:, 1, :],
                    gates_all[:, 1, :],
                    mask,
                    width_b,
                ),
            )

        updated.append(lax.cond(start <= position[-1], compute, lambda current: current, state))
    folded = tuple(updated)
    attn_a = finish(folded[0][0])
    attn_b = finish(folded[0][1])
    proj = lax.psum_scatter(
        (
            jnp.dot(attn_a, out_a, preferred_element_type=jnp.float32)
            + jnp.dot(attn_b, out_b, preferred_element_type=jnp.float32)
        ).astype(jnp.bfloat16),
        "tp",
        scatter_dimension=0,
        tiled=True,
    )
    post = rms_scale(proj.astype(jnp.float32), post_gain.astype(jnp.float32))
    mid_stream = (residual_in.astype(jnp.float32) + post).astype(jnp.bfloat16)
    normed = rms_scale(mid_stream.astype(jnp.float32), pre_gain.astype(jnp.float32)).astype(
        jnp.bfloat16
    )
    selected_count = expert_ids.shape[1]
    columns = normed.shape[1] // narrow
    slots = rows * selected_count * 5 // (4 * group_size)
    flat_experts = expert_ids.reshape(-1)
    onehot = (flat_experts[:, None] == jnp.arange(group_size, dtype=jnp.int32)[None, :]).astype(
        jnp.int32
    )
    rank = jnp.sum((jnp.cumsum(onehot, axis=0) - onehot) * onehot, axis=1)
    target = flat_experts * slots + rank
    owner = jnp.arange(rows * selected_count, dtype=jnp.int32) // selected_count
    table = jnp.full((group_size * slots,), -1, jnp.int32).at[target].set(owner)
    live = table >= 0
    source = jnp.maximum(table, 0)
    weighting = jnp.sum(
        expert_weights[:, :, None]
        * (
            target.reshape(rows, selected_count)[:, :, None]
            == jnp.arange(group_size * slots, dtype=jnp.int32)[None, None, :]
        ),
        axis=1,
    )
    column_rows = lax.all_to_all(normed, "tp", split_axis=1, concat_axis=0, tiled=True)
    outgoing = jnp.where(live[:, None], column_rows[source], jnp.zeros((), jnp.bfloat16))
    outgoing = outgoing.reshape(group_size, slots, columns)
    arrived = lax.all_to_all(outgoing, "sp", split_axis=0, concat_axis=0, tiled=True)
    flat = arrived.reshape(-1, columns)
    piece = lax.all_gather(flat, "tp", axis=1, tiled=True)
    gate_rows = w_gate[0]
    up_rows = w_up[0]
    gate = jnp.dot(piece, gate_rows, preferred_element_type=jnp.float32)
    upward = jnp.dot(piece, up_rows, preferred_element_type=jnp.float32)
    hidden_rows = (jax.nn.silu(gate) * upward).astype(jnp.bfloat16)
    hidden = hidden_rows.reshape(arrived.shape[0], arrived.shape[1], -1)
    flat_hidden = hidden.reshape(-1, hidden.shape[2])
    down_cols = w_down[0]
    summed = lax.psum_scatter(
        lax.dot_general(
            down_cols, flat_hidden, (((0,), (1,)), ((), ())), preferred_element_type=jnp.float32
        ).astype(jnp.bfloat16),
        "tp",
        scatter_dimension=0,
        tiled=True,
    )
    returned = lax.all_to_all(
        summed.reshape(columns, group_size, slots), "sp", split_axis=1, concat_axis=1, tiled=True
    )
    mixture_cols = jnp.einsum(
        "te,ce->tc",
        weighting,
        returned.reshape(columns, group_size * slots).astype(jnp.float32),
        precision=lax.Precision.HIGHEST,
    )
    mixture = lax.all_to_all(
        mixture_cols.astype(jnp.bfloat16), "tp", split_axis=0, concat_axis=1, tiled=True
    ).astype(mixture_cols.dtype)
    return (mid_stream.astype(jnp.float32) + mixture).astype(jnp.bfloat16)


def solution(mesh):
    placed = (
        P(("sp", "tp"), None),
        P("sp", "tp"),
        P("sp", "tp"),
        P("sp", "tp"),
        P("sp", "tp"),
        P("sp", "tp"),
        P("sp", "tp"),
        P("sp", None, "tp"),
        P("tp", None),
        P("tp", None),
        P(),
        P(),
        P("sp", None),
        P("sp", None),
        P("sp", None, "tp"),
        P("sp", None, "tp"),
        P("sp", "tp", None),
    )
    return jax.shard_map(
        per_device, mesh=mesh, in_specs=placed, out_specs=P(("sp", "tp"), None), check_vma=False
    )
```

profile of v0, /device:TPU:0, one launch (start us, length us, event | category | flops | bytes accessed | tf_op | source)
XLA Modules:
  0.0 352.2 jit_solution(581141033529459929)
XLA Ops:
  6.5 1.8 copy.59
  8.3 0.0 all-gather.6.cloned.1.call-update
  8.4 0.0 all-gather.8.cloned.1.call-start
  8.4 1.7 copy.60
  10.1 0.0 all-gather.10.cloned.1.call-start
  10.2 1.8 copy.61
  11.9 0.0 all-gather.10.cloned.1.call-update
  12.0 0.0 all-gather.12.cloned.1.call-start
  12.0 1.8 copy.62
  13.8 0.0 all-gather.12.cloned.1.call-update
  13.8 0.0 reduce-scatter.3.cloned.1.call-start
  13.9 0.6 slice.21
  15.0 16.0 %all_gather.19 = f32[2048,2,4]{0,2,1:T(4,128)S(1)} all-gather(f32[256,2,4]{0,2,1:T(4,128)} %param.26), channel_id=1, replica_groups=mesh['sp'=8,'tp'=4] {'sp'}, dimensions={0}, use_global_device_ids=true | all-gather | bytes 73728 | tf_op jit(solution)/shard_map/all_gather | solution.py:71
  31.0 4.8 %all-gather.6.cloned.1.call-done = bf16[2048,4,64]{0,2,1:T(8,128)(2,1)} async-done(((bf16[256,4,64]{0,2,1:T(8,128)(2,1)}), bf16[2048,4,64]{0,2,1:T(8,128)(2,1)}) %all-gather.6.cloned.1.call-update) | async-done | bytes 1048592 | tf_op jit(solution)/shard_map/all_gather | solution.py:85
  35.9 25.3 %all-gather.8.cloned.1.call-done = bf16[2048,4,64]{0,2,1:T(8,128)(2,1)} async-done(((bf16[256,4,64]{0,2,1:T(8,128)(2,1)}), bf16[2048,4,64]{0,2,1:T(8,128)(2,1)}) %all-gather.8.cloned.1.call-update) | async-done | bytes 1048592 | tf_op jit(solution)/shard_map/all_gather | solution.py:86
  61.2 31.0 %all-gather.10.cloned.1.call-done = bf16[2048,4,128]{0,2,1:T(8,128)(2,1)} async-done(((bf16[256,4,128]{0,2,1:T(8,128)(2,1)}), bf16[2048,4,128]{0,2,1:T(8,128)(2,1)}) %all-gather.10.cloned.1.call-update) | async-done | bytes 2097168 | tf_op jit(solution)/shard_map/all_gather | solution.py:87
  92.2 31.1 %all-gather.12.cloned.1.call-done = bf16[2048,4,128]{0,2,1:T(8,128)(2,1)} async-done(((bf16[256,4,128]{0,2,1:T(8,128)(2,1)}), bf16[2048,4,128]{0,2,1:T(8,128)(2,1)}) %all-gather.12.cloned.1.call-update) | async-done | bytes 2097168 | tf_op jit(solution)/shard_map/all_gather | solution.py:88
  123.3 22.6 %conditional.1 = (f32[4,256]{1,0:T(4,128)S(1)}, f32[4,256,64]{1,2,0:T(8,128)S(1)}, f32[4,256]{1,0:T(4,128)S(1)}, f32[4,256,128]{1,2,0:T(8,128)S(1)}) conditional(s32[]{:T(128)} %bitcast.9, () %tuple.13, (s32[2048]{0:T(1024)S(1)}, s32[256]{0:T(256)S(1)}, bf16[256,256]{1,0:T(8,128)(2,1)}, bf16[2048,4,64]{0,2,1:T(8,128)(2,1)}, f32[256,2,4]{0,2,1:T(4,128)}, ...), branch_computations={%region_0.0_spmd, %region_1.6_spmd} | conditional | flops 1682438144 | bytes 83133552 | solution.py:119
  123.3 0.7 slice_bitcast_fusion.3
  124.0 1.0 copy.63
  125.1 0.4 broadcast_compare_fusion
  125.4 2.7 fusion.53
  128.2 4.5 %select_reduce_fusion = (f32[4,256]{1,0:T(4,128)S(1)}, f32[4,256]{1,0:T(4,128)S(1)}, f32[4,256,2048]{2,1,0:T(8,128)S(1)}) fusion(f32[4,2048]{1,0:T(4,128)S(1)} %get-tuple-element.97, f32[4,256]{1,0:T(4,128)S(1)} %get-tuple-element.99, pred[256,2048]{1,0:T(8,128)(4,1)S(1)} %broadcast_compare_fusion, f32[4,2048]{1,0:T(4,128)S(1)} %get-tuple-element.96, ...), kind=kOutput, calls=%fused_computation.3 | convolution fusion | flops 557840384 | bytes 19742720 | tf_op jit(solution)/shard_map/cond/branch_1_fun/rhd,khd->hrk/dot_general | solution.py:24
  132.7 2.8 fusion.6
  135.5 5.9 %fusion.3 = (f32[4,256]{1,0:T(4,128)S(1)}, f32[4,256]{1,0:T(4,128)S(1)}) fusion(f32[4,256,2048]{2,1,0:T(8,128)S(1)} %get-tuple-element.100, f32[4,256]{1,0:T(4,128)S(1)} %get-tuple-element.101, f32[4,2048]{1,0:T(4,128)S(1)} %get-tuple-element.97, f32[4,256]{1,0:T(4,128)S(1)} %get-tuple-element.99, pred[256,2048]{1,0:T(8,128)(4,1)S(1)} %broadcast_compare_fusion, ...), kind=kLoop, calls=%fused_computation.11 | loop fusion | flops 25163776 | bytes 17391616 | tf_op jit(solution)/shard_map/cond/branch_1_fun/reduce_sum | solution.py:30
  141.4 4.3 %fusion.4 = f32[4,256,128]{1,2,0:T(8,128)S(1)} fusion(bf16[2048,4,128]{0,2,1:T(8,128)(2,1)} %get-tuple-element.88, f32[4,256,2048]{2,1,0:T(8,128)S(1)} %get-tuple-element.100, f32[4,256]{1,0:T(4,128)S(1)} %get-tuple-element.101, f32[4,2048]{1,0:T(4,128)S(1)} %get-tuple-element.97, f32[4,256]{1,0:T(4,128)S(1)} %get-tuple-element.99, ...), kind=kOutput, calls=%fused_computation.12 | convolution fusion | flops 549453824 | bytes 11575296 | tf_op jit(solution)/shard_map/cond | solution.py:119
  146.0 1.7 fusion.54
  147.8 1.7 fusion.29
  149.5 0.0 reduce-scatter.3.cloned.1.call-update
  149.5 0.1 copy.67
  149.7 0.1 eq.42
  149.8 0.1 eq.38
  150.0 1.1 reduce-window.6
  151.1 0.2 slice_reduce_fusion
  151.4 0.1 fusion.43
  151.5 0.1 reduce_sum.60
  151.7 0.1 mul.94
  151.8 2.4 scatter_custom_fusion
  154.3 22.3 %reduce-scatter.3.cloned.1.call-done = bf16[64,2048]{1,0:T(8,128)(2,1)} async-done(((bf16[256,2048]{1,0:T(8,128)(2,1)}), bf16[64,2048]{1,0:T(8,128)(2,1)}) %reduce-scatter.3.cloned.1.call-update) | async-done | bytes 262160 | tf_op jit(solution)/shard_map/reduce_scatter | solution.py:123
  176.6 1.1 fusion.34
  177.8 1.3 fusion.38
  179.0 0.7 copy-done.1
  179.7 0.1 fusion.40
  179.9 0.7 copy.87
  180.6 3.4 all-to-all-start
  184.0 0.0 all-gather.14.cloned.1.call-start
  184.1 0.1 broadcast_in_dim.74
  184.2 5.3 %all-to-all-done = bf16[64,4,512]{2,0,1:T(8,128)(2,1)S(1)} async-done(((bf16[64,4,512]{2,0,1:T(8,128)(2,1)}), bf16[64,4,512]{2,0,1:T(8,128)(2,1)S(1)}, u32[]{:S(2)}, u32[]{:S(2)}) %all-to-all-start) | async-done | bytes 262176 | tf_op jit(solution)/shard_map/all_to_all | solution.py:158
  189.5 2.8 gather_fusion
  192.2 0.2 broadcast_select_fusion
  192.4 22.6 %all_to_all.42 = bf16[8,80,512]{2,1,0:T(8,128)(2,1)} all-to-all(bf16[8,80,512]{2,1,0:T(8,128)(2,1)S(1)} %broadcast_select_fusion), channel_id=1, replica_groups=mesh['sp'=8,'tp'=4] {'sp'}, dimensions={0} | all-to-all | bytes 1310720 | tf_op jit(solution)/shard_map/all_to_all | solution.py:161
  215.0 0.0 all-gather.14.cloned.1.call-update
  215.1 0.0 reduce-scatter.5.cloned.1.call-start
  215.1 37.2 %all-gather.14.cloned.1.call-done = bf16[640,2048]{1,0:T(8,128)(2,1)} async-done(((bf16[640,512]{1,0:T(8,128)(2,1)}), bf16[640,2048]{1,0:T(8,128)(2,1)}) %all-gather.14.cloned.1.call-update) | async-done | bytes 2621456 | tf_op jit(solution)/shard_map/all_gather | solution.py:163
  252.4 7.4 %fusion.19 = f32[640,1024]{1,0:T(8,128)} fusion(bf16[640,2048]{1,0:T(8,128)(2,1)} %all-gather.14.cloned.1.call-done, bf16[1,2048,1024]{2,1,0:T(8,128)(2,1)} %param.34), kind=kOutput, calls=%fused_computation.32 | convolution fusion | flops 2684354560 | bytes 9437184 | tf_op jit(solution)/shard_map/dot_general | solution.py:167
  259.7 12.3 %fusion.26 = bf16[2048,640]{0,1:T(8,128)(2,1)} fusion(bf16[1,1024,2048]{2,1,0:T(8,128)(2,1)} %param.35, f32[640,1024]{1,0:T(8,128)} %fusion.19, bf16[640,2048]{1,0:T(8,128)(2,1)} %all-gather.14.cloned.1.call-done, bf16[1,2048,1024]{2,1,0:T(8,128)(2,1)} %param.33), kind=kOutput, calls=%fused_computation.37 | convolution fusion | flops 5373952000 | bytes 16252928 | tf_op jit(solution)/shard_map/dot_general | solution.py:173
  272.0 39.7 %reduce-scatter.5.cloned.1.call-done = bf16[512,640]{0,1:T(8,128)(2,1)} async-done(((bf16[2048,640]{0,1:T(8,128)(2,1)}), bf16[512,640]{0,1:T(8,128)(2,1)}) %reduce-scatter.5.cloned.1.call-update) | async-done | bytes 655376 | tf_op jit(solution)/shard_map/reduce_scatter | solution.py:172
  311.8 4.6 %all-to-all-start.2 = ((bf16[512,8,80]{0,2,1:T(8,128)(2,1)}), bf16[512,8,80]{0,2,1:T(8,128)(2,1)S(1)}, u32[]{:S(2)}, u32[]{:S(2)}) async-start(bf16[512,8,80]{0,2,1:T(8,128)(2,1)} %bitcast.106), calls=%async_computation.4 | async-start | bytes 1310720 | tf_op jit(solution)/shard_map/all_to_all | solution.py:180
  316.3 0.1 copy.70
  316.4 0.2 select_reduce_fusion.2
  316.7 17.8 %all-to-all-done.2 = bf16[512,8,80]{0,2,1:T(8,128)(2,1)S(1)} async-done(((bf16[512,8,80]{0,2,1:T(8,128)(2,1)}), bf16[512,8,80]{0,2,1:T(8,128)(2,1)S(1)}, u32[]{:S(2)}, u32[]{:S(2)}) %all-to-all-start.2) | async-done | bytes 655392 | tf_op jit(solution)/shard_map/all_to_all | solution.py:180
  334.5 0.8 convolution_convert_fusion
  335.3 8.3 %all_to_all.43 = bf16[4,64,512]{2,1,0:T(8,128)(2,1)S(1)} all-to-all(bf16[4,64,512]{2,1,0:T(8,128)(2,1)S(1)} %bitcast.104), channel_id=1, replica_groups=mesh['sp'=8,'tp'=4] {'tp'}, dimensions={0} | all-to-all | bytes 524288 | tf_op jit(solution)/shard_map/all_to_all | solution.py:189
  343.7 1.7 fusion.41
  (43 shorter events, 0.4 us)
Async XLA Ops:
  6.5 141.2 %copy-start = (bf16[512,2048]{1,0:T(8,128)(2,1)S(1)}, bf16[512,2048]{1,0:T(8,128)(2,1)}, u32[]{:S(2)}) copy-start(bf16[512,2048]{1,0:T(8,128)(2,1)} %param.28) | copy-start | bytes 6291460
  6.5 29.3 %all-gather.6.cloned.1.call-start = ((), (), s32[]{:S(2)}) async-start(), calls=%async_computation.6 | async-start | bytes 1179648 | tf_op jit(solution)/shard_map/all_gather | solution.py:85
  8.4 52.8 %all-gather.8.cloned.1.call-start = ((), (), s32[]{:S(2)}) async-start(), calls=%async_computation.7 | async-start | bytes 1179648 | tf_op jit(solution)/shard_map/all_gather | solution.py:86
  10.1 82.1 %all-gather.10.cloned.1.call-start = ((), (), s32[]{:S(2)}) async-start(), calls=%async_computation.8 | async-start | bytes 2359296 | tf_op jit(solution)/shard_map/all_gather | solution.py:87
  12.0 111.3 %all-gather.12.cloned.1.call-start = ((), (), s32[]{:S(2)}) async-start(), calls=%async_computation.9 | async-start | bytes 2359296 | tf_op jit(solution)/shard_map/all_gather | solution.py:88
  13.8 162.8 %reduce-scatter.3.cloned.1.call-start = ((), (), s32[]{:S(2)}) async-start(), calls=%async_computation.10 | async-start | bytes 1310720 | tf_op jit(solution)/shard_map/reduce_scatter | solution.py:123
  124.0 4.1 %copy-start.9 = (bf16[256,512]{1,0:T(8,128)(2,1)S(1)}, bf16[256,512]{1,0:T(8,128)(2,1)}, u32[]{:S(2)}) copy-start(bf16[256,512]{1,0:T(8,128)(2,1)} %get-tuple-element.48) | copy-start | bytes 786436 | tf_op jit(solution)/shard_map/cond
  125.1 3.1 copy-start.7
  128.2 4.5 %copy-start.8 = (bf16[2048,4,64]{0,2,1:T(8,128)(2,1)S(1)}, bf16[2048,4,64]{0,2,1:T(8,128)(2,1)}, u32[]{:S(2)}) copy-start(bf16[2048,4,64]{0,2,1:T(8,128)(2,1)} %get-tuple-element.33) | copy-start | bytes 3145732 | tf_op jit(solution)/shard_map/cond
  145.9 3.6 %copy-start.5 = (s32[256,2]{0,1:T(2,128)S(1)}, s32[256,2]{0,1:T(2,128)}, u32[]{:S(2)}) copy-start(s32[256,2]{0,1:T(2,128)} %param.31) | copy-start | bytes 6148
  146.0 4.0 %copy-start.3 = (bf16[2048]{0:T(1024)(128)(2,1)S(1)}, bf16[2048]{0:T(1024)(128)(2,1)}, u32[]{:S(2)}) copy-start(bf16[2048]{0:T(1024)(128)(2,1)} %param.29) | copy-start | bytes 12292
  146.0 4.0 %copy-start.4 = (bf16[2048]{0:T(1024)(128)(2,1)S(1)}, bf16[2048]{0:T(1024)(128)(2,1)}, u32[]{:S(2)}) copy-start(bf16[2048]{0:T(1024)(128)(2,1)} %param.30) | copy-start | bytes 12292
  146.0 31.7 %copy-start.2 = (bf16[64,2048]{1,0:T(8,128)(2,1)S(1)}, bf16[64,2048]{1,0:T(8,128)(2,1)}, u32[]{:S(2)}) copy-start(bf16[64,2048]{1,0:T(8,128)(2,1)} %param.19) | copy-start | bytes 786436
  179.0 0.7 copy-start.1
  180.6 8.9 %all-to-all-start = ((bf16[64,4,512]{2,0,1:T(8,128)(2,1)}), bf16[64,4,512]{2,0,1:T(8,128)(2,1)S(1)}, u32[]{:S(2)}, u32[]{:S(2)}) async-start(bf16[64,4,512]{2,0,1:T(8,128)(2,1)} %bitcast.94), calls=%async_computation.1 | async-start | bytes 524288 | tf_op jit(solution)/shard_map/all_to_all | solution.py:158
  184.0 68.3 %all-gather.14.cloned.1.call-start = ((), (), s32[]{:S(2)}) async-start(), calls=%async_computation.11 | async-start | bytes 3276800 | tf_op jit(solution)/shard_map/all_gather | solution.py:163
  215.1 96.7 %reduce-scatter.5.cloned.1.call-start = ((), (), s32[]{:S(2)}) async-start(), calls=%async_computation.12 | async-start | bytes 3276800 | tf_op jit(solution)/shard_map/reduce_scatter | solution.py:172
  259.7 56.7 %copy-start.6 = (f32[256,2]{0,1:T(2,128)S(1)}, f32[256,2]{0,1:T(2,128)}, u32[]{:S(2)}) copy-start(f32[256,2]{0,1:T(2,128)} %param.32) | copy-start | bytes 6148
  311.8 22.7 %all-to-all-start.2 = ((bf16[512,8,80]{0,2,1:T(8,128)(2,1)}), bf16[512,8,80]{0,2,1:T(8,128)(2,1)S(1)}, u32[]{:S(2)}, u32[]{:S(2)}) async-start(bf16[512,8,80]{0,2,1:T(8,128)(2,1)} %bitcast.106), calls=%async_computation.4 | async-start | bytes 1310720 | tf_op jit(solution)/shard_map/all_to_all | solution.py:180
Sparse Core Ops, SparseCore 0:
  8.9 26.9 all-gather.5
  37.5 23.6 all-gather.7
  62.8 29.3 all-gather.9
  93.6 29.6 all-gather.11
  149.6 26.9 reduce-scatter.2
  215.2 37.1 all-gather.13
  272.2 39.5 reduce-scatter.4
where the time goes:
time: 353 us; the launch traced here: 352 us
  waiting for transfers between devices  215 us (61%)
  blocking collectives  46.9 us (13%)
  matrix products  38.2 us (11%)
  local copies, waits for them, and re-layouts  17.2 us (5%)
  between operations  14.4 us (4%)
  other arithmetic  12.3 us (3%)
  starting transfers between devices  8.24 us (2%)
    reduce_scatter x1, waiting for transfers between devices, per_device(): lax.psum_scatter(lax.dot_general(down_cols, flat_hidden, (((0,), (1,)), (...  39.7 us
    all_gather x1, waiting for transfers between devices, per_device(): piece = lax.all_gather(flat, 'tp', axis=1, tiled=True)  37.2 us
    all_gather x1, waiting for transfers between devices, per_device(): lax.all_gather(value_b.reshape(rows, heads, width_b), 'sp', axis=0, tiled...  31.1 us
    all_gather x1, waiting for transfers between devices, per_device(): lax.all_gather(key_b.reshape(rows, heads, width_b), 'sp', axis=0, tiled=T...  31 us
    all_gather x1, waiting for transfers between devices, per_device(): lax.all_gather(value_a.reshape(rows, heads, width_a), 'sp', axis=0, tiled...  25.3 us
    all_to_all x1, blocking collectives, per_device(): lax.all_to_all(outgoing, 'sp', split_axis=0, concat_axis=0, tiled=True)  22.6 us
    reduce_scatter x1, waiting for transfers between devices, per_device(): lax.psum_scatter((jnp.dot(attn_a, out_a, preferred_element_type=jnp.float...  22.3 us
    all_to_all x1, waiting for transfers between devices, per_device(): lax.all_to_all(summed.reshape(columns, group_size, slots), 'sp', split_ax...  17.8 us
  transfers between devices with their start and end apart: 9, of which 9 were waited for; matrix products, arithmetic and copies ran while one was open for 3% of the time, Pallas kernels for 0%

commit v1 on v0

v1 whole, which is shorter than its diff:
```python
import functools

import jax
import jax.numpy as jnp
from jax import lax
from jax.experimental import pallas as pl
from jax.experimental.pallas import tpu as pltpu
from jax.sharding import PartitionSpec as P

eps_norm = 1e-06
big_neg = -1e30


def rms_scale(values, gain):
    return values * lax.rsqrt(jnp.mean(values * values, axis=-1, keepdims=True) + eps_norm) * gain


def empty_state(item_count, heads, width):
    return (
        jnp.full((heads, item_count), big_neg, jnp.float32),
        jnp.zeros((heads, item_count), jnp.float32),
        jnp.zeros((heads, item_count, width), jnp.float32),
    )


def update_state(state, query, key_rows, values, query_gate, key_gate, mask, width):
    highest, total, accum = state
    score = jnp.einsum(
        "rhd,khd->hrk", query, key_rows, preferred_element_type=jnp.float32
    ) * width ** (-0.5)
    score = score + query_gate.T[:, :, None] - key_gate.T[:, None, :]
    new_high = jnp.maximum(highest, jnp.max(jnp.where(mask[None], score, big_neg), axis=2))
    expo = jnp.exp(jnp.where(mask[None], score - new_high[:, :, None], big_neg))
    total = jnp.sum(expo, axis=2)
    accum = jnp.einsum(
        "hrk,khd->hrd", expo.astype(jnp.bfloat16), values, preferred_element_type=jnp.float32
    )
    return (new_high, total, accum)


def finish(state):
    highest, total, accum = state
    heads, item_count, width = accum.shape
    result = accum / total[:, :, None]
    return result.transpose(1, 0, 2).reshape(item_count, heads * width).astype(jnp.bfloat16)


def exchange_kernel(axis, count, plans, *refs):
    arrays = len(plans)
    ins, outs = refs[:arrays], refs[arrays : 2 * arrays]
    send_sem, recv_sem, own_sem = refs[2 * arrays :]
    me = lax.axis_index(axis)

    barrier = pltpu.get_barrier_semaphore()
    for step in range(1, count):
        pl.semaphore_signal(
            barrier,
            inc=1,
            device_id={axis: lax.rem(me + step, count)},
            device_id_type=pl.DeviceIdType.MESH,
        )
    pl.semaphore_wait(barrier, count - 1)

    def remote(index, step, peer, sender):
        source, target, _ = plans[index]
        return pltpu.make_async_remote_copy(
            src_ref=source(ins[index], peer),
            dst_ref=target(outs[index], sender),
            send_sem=send_sem.at[index, step],
            recv_sem=recv_sem.at[index, step],
            device_id={axis: peer},
            device_id_type=pl.DeviceIdType.MESH,
        )

    def own(index):
        source, target, _ = plans[index]
        return pltpu.make_async_copy(
            source(ins[index], me), target(outs[index], me), own_sem.at[index]
        )

    def guarded(least, who, action):
        if least:
            pl.when(who >= least)(action)
        else:
            action()

    for step in range(1, count):
        peer = lax.rem(me + step, count)
        for index in range(arrays):
            guarded(
                plans[index][2], peer, lambda: remote(index, step, peer, me).start()
            )
    for index in range(arrays):
        guarded(plans[index][2], me, lambda: own(index).start())
    for index in range(arrays):
        guarded(plans[index][2], me, lambda: own(index).wait())
    for step in range(1, count):
        peer = lax.rem(me + step, count)
        sender = lax.rem(me + count - step, count)
        for index in range(arrays):
            guarded(
                plans[index][2], me, lambda: remote(index, step, peer, sender).wait_recv()
            )
            guarded(
                plans[index][2], peer, lambda: remote(index, step, peer, me).wait_send()
            )


def exchange(values, shapes, plans, axis, name):
    count = lax.axis_size(axis)
    arrays = len(values)
    result = pl.pallas_call(
        functools.partial(exchange_kernel, axis, count, plans),
        out_shape=[
            jax.ShapeDtypeStruct(shape, value.dtype) for shape, value in zip(shapes, values)
        ],
        in_specs=[pl.BlockSpec(memory_space=pltpu.VMEM)] * arrays,
        out_specs=[pl.BlockSpec(memory_space=pltpu.VMEM)] * arrays,
        scratch_shapes=[
            pltpu.SemaphoreType.DMA((arrays, count)),
            pltpu.SemaphoreType.DMA((arrays, count)),
            pltpu.SemaphoreType.DMA((arrays,)),
        ],
        compiler_params=pltpu.CompilerParams(collective_id=name, has_side_effects=True),
    )(*values)
    return result


def item(ref, index):
    return ref.at[index]


def whole_ref(ref, index):
    return ref


def column_block(width):
    return lambda ref, index: ref.at[:, pl.ds(pl.multiple_of(index * width, width), width)]


def row_block(height):
    return lambda ref, index: ref.at[pl.ds(pl.multiple_of(index * height, height), height), :]


def attend_kernel(block, scale_ref, query_ref, key_ref, value_ref, row_ref, col_ref, out_ref):
    scale = scale_ref[0]
    total_rows = query_ref.shape[0]
    lower = lax.broadcasted_iota(jnp.int32, (block, block), 1) <= lax.broadcasted_iota(
        jnp.int32, (block, block), 0
    )
    dims = (((1,), (1,)), ((), ()))
    for start in range(0, total_rows, block):
        here = slice(start, start + block)
        query = query_ref[here, :]
        gate = col_ref[here, :]
        diag = lax.dot_general(query, key_ref[here, :], dims, preferred_element_type=jnp.float32)
        diag = diag * scale + gate - row_ref[0:1, here]
        diag = jnp.where(lower, diag, big_neg)
        highest = jnp.max(diag, axis=1, keepdims=True)
        if start:
            early = slice(0, start)
            score = lax.dot_general(
                query, key_ref[early, :], dims, preferred_element_type=jnp.float32
            )
            score = score * scale + gate - row_ref[0:1, early]
            highest = jnp.maximum(highest, jnp.max(score, axis=1, keepdims=True))
        expo = jnp.exp(diag - highest)
        total = jnp.sum(expo, axis=1, keepdims=True)
        mixed = jnp.dot(
            expo.astype(jnp.bfloat16), value_ref[here, :], preferred_element_type=jnp.float32
        )
        if start:
            expo = jnp.exp(score - highest)
            total = total + jnp.sum(expo, axis=1, keepdims=True)
            mixed = mixed + jnp.dot(
                expo.astype(jnp.bfloat16), value_ref[early, :], preferred_element_type=jnp.float32
            )
        out_ref[here, :] = (mixed / total).astype(jnp.bfloat16)


def headwise_attention(
    query_a, key_a, value_a, query_b, key_b, value_b, cum_gates
):
    rows = query_a.shape[0]
    heads = cum_gates.shape[2]
    width_a = query_a.shape[1] // heads
    width_b = query_b.shape[1] // heads
    count = lax.axis_size("sp")
    me = lax.axis_index("sp")

    def split(values, width):
        return values.reshape(rows, heads, width).transpose(1, 0, 2)

    pad = jnp.zeros((heads, rows, 2 * width_b - 3 * width_a), jnp.bfloat16)
    first = jnp.concatenate(
        [split(query_a, width_a), split(key_a, width_a), split(value_a, width_a), pad], axis=2
    )
    second = jnp.concatenate([split(query_b, width_b), split(key_b, width_b)], axis=2)
    packed = jnp.concatenate([first, second], axis=0)
    late = split(value_b, width_b)
    gates = cum_gates.transpose(1, 2, 0).reshape(2 * heads, 1, rows)
    gates = jnp.broadcast_to(gates, (2 * heads, 8, rows))
    main, tail, gate_rows = exchange(
        [packed, late, gates],
        [
            (count * rows, 2 * width_b),
            (count * rows, width_b),
            (8, count * rows),
        ],
        [
            (item, row_block(rows), 0),
            (lambda ref, index: ref.at[jnp.maximum(index - heads, 0)], row_block(rows), heads),
            (item, column_block(rows), 0),
        ],
        "sp",
        1,
    )
    narrow_head = me < heads
    fill = jnp.zeros((count * rows, width_b - width_a), jnp.bfloat16)

    def widen(index):
        return jnp.concatenate([main[:, index * width_a : (index + 1) * width_a], fill], axis=1)

    query = jnp.where(narrow_head, widen(0), main[:, :width_b])
    keys = jnp.where(narrow_head, widen(1), main[:, width_b:])
    values = jnp.where(narrow_head, widen(2), tail)
    scale = jnp.where(narrow_head, width_a ** (-0.5), width_b ** (-0.5)).astype(jnp.float32)
    mixed = pl.pallas_call(
        functools.partial(attend_kernel, rows),
        out_shape=jax.ShapeDtypeStruct((count * rows, width_b), jnp.bfloat16),
        in_specs=[pl.BlockSpec(memory_space=pltpu.SMEM)]
        + [pl.BlockSpec(memory_space=pltpu.VMEM)] * 5,
        out_specs=pl.BlockSpec(memory_space=pltpu.VMEM),
    )(scale.reshape(1), query, keys, values, gate_rows, gate_rows[0].reshape(-1, 1))
    (back,) = exchange(
        [mixed], [(count, rows, width_b)], [(row_block(rows), item, 0)], "sp", 2
    )
    attn_a = back[:heads, :, :width_a].transpose(1, 0, 2).reshape(rows, heads * width_a)
    attn_b = back[heads:].transpose(1, 0, 2).reshape(rows, heads * width_b)
    return attn_a, attn_b


def gathered_attention(
    query_a, key_a, value_a, query_b, key_b, value_b, cum_gates
):
    rows = query_a.shape[0]
    heads = cum_gates.shape[2]
    width_a = query_a.shape[1] // heads
    width_b = query_b.shape[1] // heads
    here = lax.axis_index("sp")
    offset = here * rows
    gates_all = lax.all_gather(cum_gates, "sp", axis=0, tiled=True)
    queries_a = query_a.reshape(rows, heads, width_a)
    queries_b = query_b.reshape(rows, heads, width_b)
    blocks = [(queries_a, queries_b, offset + jnp.arange(rows, dtype=jnp.int32), cum_gates)]
    initial = tuple(
        (
            (
                empty_state(block[2].shape[0], heads, width_a),
                empty_state(block[2].shape[0], heads, width_b),
            )
            for block in blocks
        )
    )
    start = jnp.int32(0)
    piece_key_a = lax.all_gather(key_a.reshape(rows, heads, width_a), "sp", axis=0, tiled=True)
    piece_value_a = lax.all_gather(value_a.reshape(rows, heads, width_a), "sp", axis=0, tiled=True)
    piece_key_b = lax.all_gather(key_b.reshape(rows, heads, width_b), "sp", axis=0, tiled=True)
    piece_value_b = lax.all_gather(value_b.reshape(rows, heads, width_b), "sp", axis=0, tiled=True)
    item_count = piece_key_a.shape[0]
    key_pos = jnp.arange(item_count, dtype=jnp.int32)
    updated = []
    for state, (block_a, block_b, position, block_gate) in zip(initial, blocks):

        def compute(current):
            mask = key_pos[None, :] <= position[:, None]
            return (
                update_state(
                    current[0],
                    block_a,
                    piece_key_a,
                    piece_value_a,
                    block_gate[:, 0, :],
                    gates_all[:, 0, :],
                    mask,
                    width_a,
                ),
                update_state(
                    current[1],
                    block_b,
                    piece_key_b,
                    piece_value_b,
                    block_gate[:, 1, :],
                    gates_all[:, 1, :],
                    mask,
                    width_b,
                ),
            )

        updated.append(lax.cond(start <= position[-1], compute, lambda current: current, state))
    folded = tuple(updated)
    attn_a = finish(folded[0][0])
    attn_b = finish(folded[0][1])
    return attn_a, attn_b


def per_device(
    residual_in,
    query_a,
    key_a,
    value_a,
    query_b,
    key_b,
    value_b,
    cum_gates,
    out_a,
    out_b,
    post_gain,
    pre_gain,
    expert_ids,
    expert_weights,
    w_gate,
    w_up,
    w_down,
):
    rows = query_a.shape[0]
    heads = cum_gates.shape[2]
    width_a = query_a.shape[1] // heads
    width_b = query_b.shape[1] // heads
    group_size = lax.axis_size("sp")
    narrow = lax.axis_size("tp")
    columns = out_a.shape[1] // narrow
    own_rows = rows // narrow
    fits = 2 * heads == group_size and 2 * width_b >= 3 * width_a and width_b >= width_a
    attention = headwise_attention if fits else gathered_attention
    attn_a, attn_b = attention(query_a, key_a, value_a, query_b, key_b, value_b, cum_gates)
    part = (
        jnp.dot(attn_a, out_a, preferred_element_type=jnp.float32)
        + jnp.dot(attn_b, out_b, preferred_element_type=jnp.float32)
    ).astype(jnp.bfloat16)
    (parts,) = exchange(
        [part],
        [(narrow, own_rows, part.shape[1])],
        [(row_block(own_rows), item, 0)],
        "tp",
        3,
    )
    proj = jnp.sum(parts.astype(jnp.float32), axis=0).astype(jnp.bfloat16)
    post = rms_scale(proj.astype(jnp.float32), post_gain.astype(jnp.float32))
    mid_stream = (residual_in.astype(jnp.float32) + post).astype(jnp.bfloat16)
    normed = rms_scale(mid_stream.astype(jnp.float32), pre_gain.astype(jnp.float32)).astype(
        jnp.bfloat16
    )
    selected_count = expert_ids.shape[1]
    slots = rows * selected_count * 5 // (4 * group_size)
    named = expert_ids[:, :, None] == jnp.arange(group_size, dtype=jnp.int32)
    position = jnp.arange(rows, dtype=jnp.int32)
    before = (position[None, :] < position[:, None]).astype(jnp.bfloat16)
    earlier = jnp.dot(
        before, jnp.any(named, axis=1).astype(jnp.bfloat16), preferred_element_type=jnp.float32
    ).astype(jnp.int32)
    rank = jnp.sum(jnp.where(named, earlier[:, None, :], 0), axis=2)
    target = expert_ids * slots + rank
    chosen = target[:, :, None] == jnp.arange(group_size * slots, dtype=jnp.int32)
    weighting = jnp.sum(jnp.where(chosen, expert_weights[:, :, None], 0.0), axis=1)
    placing = jnp.any(chosen, axis=1).astype(jnp.bfloat16)
    (column_rows,) = exchange(
        [normed],
        [(rows, columns)],
        [(column_block(columns), row_block(own_rows), 0)],
        "tp",
        4,
    )
    outgoing = lax.dot_general(
        placing, column_rows, (((0,), (0,)), ((), ())), preferred_element_type=jnp.float32
    ).astype(jnp.bfloat16)
    outgoing = outgoing.reshape(group_size, slots, columns)
    (arrived,) = exchange(
        [outgoing], [(group_size, slots, columns)], [(item, item, 0)], "sp", 5
    )
    (piece,) = exchange(
        [arrived.reshape(-1, columns)],
        [(group_size * slots, columns * narrow)],
        [(whole_ref, column_block(columns), 0)],
        "tp",
        6,
    )
    gate = jnp.dot(piece, w_gate[0], preferred_element_type=jnp.float32)
    upward = jnp.dot(piece, w_up[0], preferred_element_type=jnp.float32)
    hidden = (jax.nn.silu(gate) * upward).astype(jnp.bfloat16)
    down = jnp.dot(hidden, w_down[0], preferred_element_type=jnp.float32).astype(jnp.bfloat16)
    (downs,) = exchange(
        [down],
        [(narrow, group_size * slots, columns)],
        [(column_block(columns), item, 0)],
        "tp",
        7,
    )
    summed = jnp.sum(downs.astype(jnp.float32), axis=0).astype(jnp.bfloat16)
    (returned,) = exchange(
        [summed.reshape(group_size, slots, columns)],
        [(group_size, slots, columns)],
        [(item, item, 0)],
        "sp",
        8,
    )
    mixture_cols = jnp.dot(
        weighting,
        returned.reshape(group_size * slots, columns).astype(jnp.float32),
        precision=lax.Precision.HIGHEST,
    )
    (mixture,) = exchange(
        [mixture_cols.astype(jnp.bfloat16)],
        [(own_rows, columns * narrow)],
        [(row_block(own_rows), column_block(columns), 0)],
        "tp",
        9,
    )
    return (mid_stream.astype(jnp.float32) + mixture.astype(jnp.float32)).astype(jnp.bfloat16)


def solution(mesh):
    placed = (
        P(("sp", "tp"), None),
        P("sp", "tp"),
        P("sp", "tp"),
        P("sp", "tp"),
        P("sp", "tp"),
        P("sp", "tp"),
        P("sp", "tp"),
        P("sp", None, "tp"),
        P("tp", None),
        P("tp", None),
        P(),
        P(),
        P("sp", None),
        P("sp", None),
        P("sp", None, "tp"),
        P("sp", None, "tp"),
        P("sp", "tp", None),
    )
    return jax.shard_map(
        per_device, mesh=mesh, in_specs=placed, out_specs=P(("sp", "tp"), None), check_vma=False
    )
```

time: 353 us -> 266 us (0.75)
  waiting for transfers between devices: 215 us -> 0 us
  Pallas kernels: 0 us -> 207 us
  blocking collectives: 46.9 us -> 0 us
  between operations: 14.4 us -> 0.33 us
  starting transfers between devices: 8.24 us -> 0 us
  matrix products: 38.2 us -> 30.9 us
  local copies, waits for them, and re-layouts: 17.2 us -> 13 us
    pallas_call x0 -> x10, Pallas kernels: none -> 207 us  [the longest x9 200 us: exchange(): pl.pallas_call(functools.partial(exchange_kernel, axis, count, plans), ou...]
    all_gather x5 -> x0, waiting for transfers between devices: 130 us -> none  [the longest x1 37.2 us: per_device(): piece = lax.all_gather(flat, 'tp', axis=1, tiled=True)]
    reduce_scatter x2 -> x0, waiting for transfers between devices: 62 us -> none  [the longest x1 39.7 us: per_device(): lax.psum_scatter(lax.dot_general(down_cols, flat_hidden, (((0,), (1,)), (...]
    all_to_all x2 -> x0, blocking collectives: 30.9 us -> none  [the longest x1 22.6 us: per_device(): lax.all_to_all(outgoing, 'sp', split_axis=0, concat_axis=0, tiled=True)]
    all_to_all x2 -> x0, waiting for transfers between devices: 23.1 us -> none  [the longest x1 17.8 us: per_device(): lax.all_to_all(summed.reshape(columns, group_size, slots), 'sp', split_ax...]
    all_gather x1 -> x0, blocking collectives: 16 us -> none  [per_device(): gates_all = lax.all_gather(cum_gates, 'sp', axis=0, tiled=True)]
    all_to_all x2 -> x0, starting transfers between devices: 7.99 us -> none  [the longest x1 4.58 us: per_device(): lax.all_to_all(summed.reshape(columns, group_size, slots), 'sp', split_ax...]
    dot_general x6 -> x5, matrix products: 30.4 us -> 24.6 us  [the longest x1 12.3 us: per_device(): jnp.dot(hidden, w_down[0], preferred_element_type=jnp.float32)]
  transfers between devices with their start and end apart: 9 -> 0, of which waited for: 9 -> 0; matrix products, arithmetic and copies ran while one was open for 3% -> 0% of each run, Pallas kernels for 0% -> 0%
where the time goes in v1:
time: 266 us; the launch traced here: 264 us
  Pallas kernels  207 us (78%)
  matrix products  30.9 us (12%)
  local copies, waits for them, and re-layouts  13 us (5%)
  other arithmetic  12.2 us (5%)
    pallas_call x9, Pallas kernels, exchange(): pl.pallas_call(functools.partial(exchange_kernel, axis, count, plans), ou...  200 us
    dot_general x1, matrix products, per_device(): jnp.dot(hidden, w_down[0], preferred_element_type=jnp.float32)  12.3 us
    pallas_call x1, Pallas kernels, headwise_attention(): pl.pallas_call(functools.partial(attend_kernel, rows), out_shape=jax.Shap...  7.63 us
    dot_general x1, matrix products, per_device(): upward = jnp.dot(piece, w_up[0], preferred_element_type=jnp.float32)  7.36 us

profile of v1, /device:TPU:0, one launch (start us, length us, event | category | flops | bytes accessed | tf_op | source)
XLA Modules:
  0.0 263.7 jit_solution(15475110468602041166)
XLA Ops:
  0.0 0.0 copy-start
  0.0 1.2 copy.49
  1.2 0.2 copy.50
  1.4 1.1 copy.47
  2.5 0.2 copy.48
  2.7 1.0 copy.41
  3.7 0.0 copy-start.7
  3.7 0.2 copy.42
  3.9 0.0 copy-done.4
  3.9 0.1 copy.43
  4.0 0.2 copy.44
  4.2 0.0 copy-done.5
  4.2 0.1 copy.45
  4.3 0.2 copy.46
  4.5 0.1 pad.6.clone
  4.6 1.4 maximum_maximum_fusion.refs_0_
  6.0 1.1 copy.51
  7.1 0.8 copy.52
  7.9 0.0 copy-done.7
  7.9 0.6 broadcast_in_dim.28.refs_2_
  8.6 32.1 %shard_map.163 = (bf16[2048,256]{1,0:T(8,128)(2,1)}, bf16[2048,128]{1,0:T(8,128)(2,1)}, f32[8,2048]{1,0:T(8,128)}) custom-call(bf16[8,256,256]{2,1,0:T(8,128)(2,1)} %maximum_maximum_fusion.refs_0_, bf16[4,256,128]{2,1,0:T(8,128)(2,1)} %bitcast.64, f32[8,8,256]{2,1,0:T(8,128)} %broadcast_in_dim.28.refs_2_), custom_call_target="tpu_custom_call" | custom-call | tf_op jit(solution)/shard_map/pallas_call | solution.py:112
  40.7 0.0 copy-start.1
  40.7 2.4 fusion.26
  43.1 0.0 copy-done.11
  43.1 0.0 copy-done.1
  43.1 2.7 %slice_select_fusion = (bf16[2048,128]{1,0:T(8,128)(2,1)}, bf16[2048,128]{1,0:T(8,128)(2,1)}, bf16[2048,128]{1,0:T(8,128)(2,1)}) fusion(bf16[2048,256]{1,0:T(8,128)(2,1)S(1)} %copy-done.1, bf16[2048,64]{1,0:T(8,128)(2,1)} %get-tuple-element.14, pred[]{:T(512)S(6)} %lt.16, pred[128]{0:T(512)(128)(4,1)S(1)} %copy-done.11, ...), kind=kLoop, calls=%fused_computation.32 | loop fusion | flops 1048576 | bytes 3670145 | tf_op jit(solution)/shard_map/jit(_where)/select_n | solution.py:225
  45.8 0.8 slice_bitcast_fusion.2
  46.7 1.4 copy.53.col_ref
  48.0 7.6 %shard_map.164.refs_0_ = bf16[2048,128]{1,0:T(8,128)(2,1)} custom-call(f32[1]{0:T(128)} %bitcast.scale_ref, bf16[2048,128]{1,0:T(8,128)(2,1)} %get-tuple-element.16.query_ref, bf16[2048,128]{1,0:T(8,128)(2,1)} %get-tuple-element.15.key_ref, bf16[2048,128]{1,0:T(8,128)(2,1)} %get-tuple-element.17.value_ref, f32[8,2048]{1,0:T(8,128)} %get-tuple-element.10.row_ref, ...), custom_call_target="tpu_custom_call" | custom-call | tf_op jit(solution)/shard_map/pallas_call | solution.py:228
  55.7 25.5 %shard_map.165 = bf16[8,256,128]{2,1,0:T(8,128)(2,1)} custom-call(bf16[2048,128]{1,0:T(8,128)(2,1)} %shard_map.164.refs_0_), custom_call_target="tpu_custom_call" | custom-call | tf_op jit(solution)/shard_map/pallas_call | solution.py:112
  81.2 0.0 copy-start.2
  81.2 1.0 slice_bitcast_fusion.1
  82.2 0.1 copy.54
  82.4 3.0 %fusion.27 = f32[256,2048]{1,0:T(8,128)} fusion(bf16[256,256]{0,1:T(8,128)(2,1)S(1)} %bitcast.66, bf16[256,2048]{1,0:T(8,128)(2,1)} %param.25), kind=kOutput, calls=%fused_computation.45 | convolution fusion | flops 268435456 | bytes 3276800 | tf_op jit(solution)/shard_map/dot_general | solution.py:338
  85.4 0.0 copy-done.2
  85.4 0.1 copy.55
  85.6 0.0 copy-done
  85.6 3.3 %fusion.9.refs_0_ = bf16[256,2048]{1,0:T(8,128)(2,1)} fusion(f32[256,2048]{1,0:T(8,128)} %fusion.27, bf16[256,512]{0,1:T(8,128)(2,1)S(1)} %bitcast.65, bf16[512,2048]{1,0:T(8,128)(2,1)S(1)} %copy-done), kind=kOutput, calls=%fused_computation.9 | convolution fusion | flops 537919488 | bytes 5505024 | tf_op jit(solution)/shard_map/dot_general | solution.py:339
  88.9 17.8 %shard_map.166 = bf16[4,64,2048]{2,1,0:T(8,128)(2,1)} custom-call(bf16[256,2048]{1,0:T(8,128)(2,1)} %fusion.9.refs_0_), custom_call_target="tpu_custom_call" | custom-call | tf_op jit(solution)/shard_map/pallas_call | solution.py:112
  106.8 1.4 reduce_sum.60
  108.2 0.2 fusion.15
  108.3 0.0 copy-done.8
  108.3 0.0 copy-done.3
  108.4 0.3 fusion.19
  108.7 0.0 copy-done.9
  108.7 0.8 fusion.21.refs_0_
  109.5 8.1 %shard_map.167 = bf16[256,512]{1,0:T(8,128)(2,1)} custom-call(bf16[64,2048]{1,0:T(8,128)(2,1)} %fusion.21.refs_0_), custom_call_target="tpu_custom_call" | custom-call | tf_op jit(solution)/shard_map/pallas_call | solution.py:112
  117.6 0.0 copy-done.6
  117.6 0.2 convolution_convert_fusion.2
  117.8 0.2 fusion.12
  118.0 2.2 convolution_convert_fusion
  120.2 18.5 %shard_map.168 = bf16[8,80,512]{2,1,0:T(8,128)(2,1)} custom-call(bf16[8,80,512]{2,1,0:T(8,128)(2,1)} %bitcast.53), custom_call_target="tpu_custom_call" | custom-call | tf_op jit(solution)/shard_map/pallas_call | solution.py:112
  138.7 34.7 %shard_map.169 = bf16[640,2048]{1,0:T(8,128)(2,1)} custom-call(bf16[640,512]{1,0:T(8,128)(2,1)} %bitcast.55), custom_call_target="tpu_custom_call" | custom-call | tf_op jit(solution)/shard_map/pallas_call | solution.py:112
  173.5 7.4 %fusion.2 = f32[640,1024]{1,0:T(8,128)} fusion(bf16[640,2048]{1,0:T(8,128)(2,1)} %shard_map.169, bf16[1,2048,1024]{2,1,0:T(8,128)(2,1)} %param.32), kind=kOutput, calls=%fused_computation.2 | convolution fusion | flops 2684354560 | bytes 9437184 | tf_op jit(solution)/shard_map/dot_general | solution.py:389
  180.9 12.3 %fusion.6.refs_0_ = bf16[640,2048]{1,0:T(8,128)(2,1)} fusion(bf16[1,1024,2048]{2,1,0:T(8,128)(2,1)} %param.33, f32[640,1024]{1,0:T(8,128)} %fusion.2, bf16[640,2048]{1,0:T(8,128)(2,1)} %shard_map.169, bf16[1,2048,1024]{2,1,0:T(8,128)(2,1)} %param.31), kind=kOutput, calls=%fused_computation.6 | convolution fusion | flops 5373952000 | bytes 16252928 | tf_op jit(solution)/shard_map/dot_general | solution.py:391
  193.2 35.0 %shard_map.170 = bf16[4,640,512]{2,1,0:T(8,128)(2,1)} custom-call(bf16[640,2048]{1,0:T(8,128)(2,1)} %fusion.6.refs_0_), custom_call_target="tpu_custom_call" | custom-call | tf_op jit(solution)/shard_map/pallas_call | solution.py:112
  228.2 0.0 copy-start.10
  228.2 3.2 %reduce_sum.65 = bf16[640,512]{1,0:T(8,128)(2,1)} reduce(bf16[4,640,512]{2,1,0:T(8,128)(2,1)} %shard_map.170, bf16[]{:T(256)} %constant.28.clone.1), dimensions={0}, to_apply=%region_7.8 | reduce | flops 983040 | bytes 3276802 | tf_op jit(solution)/shard_map/reduce_sum | solution.py:399
  231.4 19.1 %shard_map.171 = bf16[8,80,512]{2,1,0:T(8,128)(2,1)} custom-call(bf16[8,80,512]{2,1,0:T(8,128)(2,1)} %bitcast.54), custom_call_target="tpu_custom_call" | custom-call | tf_op jit(solution)/shard_map/pallas_call | solution.py:112
  250.5 0.0 copy-done.10
  250.5 0.2 select_reduce_fusion
  250.7 2.6 convolution_convert_fusion.1.refs_0_
  253.3 8.7 %shard_map.172 = bf16[64,2048]{1,0:T(8,128)(2,1)} custom-call(bf16[256,512]{1,0:T(8,128)(2,1)} %convolution_convert_fusion.1.refs_0_), custom_call_target="tpu_custom_call" | custom-call | tf_op jit(solution)/shard_map/pallas_call | solution.py:112
  262.0 1.7 fusion.22
  (17 shorter events, 0.1 us)
Async XLA Ops:
  0.0 85.6 %copy-start = (bf16[512,2048]{1,0:T(8,128)(2,1)S(1)}, bf16[512,2048]{1,0:T(8,128)(2,1)}, u32[]{:S(2)}) copy-start(bf16[512,2048]{1,0:T(8,128)(2,1)} %param.26) | copy-start | bytes 6291460
  0.0 3.9 %copy-start.4 = (bf16[256,256]{1,0:T(8,128)(2,1)S(1)}, bf16[256,256]{1,0:T(8,128)(2,1)}, u32[]{:S(2)}) copy-start(bf16[256,256]{1,0:T(8,128)(2,1)} %param.19) | copy-start | bytes 393220
  0.0 4.2 %copy-start.5 = (bf16[256,256]{1,0:T(8,128)(2,1)S(1)}, bf16[256,256]{1,0:T(8,128)(2,1)}, u32[]{:S(2)}) copy-start(bf16[256,256]{1,0:T(8,128)(2,1)} %param.20) | copy-start | bytes 393220
  3.7 4.2 %copy-start.7 = (f32[256,2,4]{0,2,1:T(4,128)S(1)}, f32[256,2,4]{0,2,1:T(4,128)}, u32[]{:S(2)}) copy-start(f32[256,2,4]{0,2,1:T(4,128)} %param.24) | copy-start | bytes 24580
  6.0 37.1 %copy-start.11 = (pred[128]{0:T(512)(128)(4,1)S(1)}, pred[128]{0:T(512)(128)(4,1)}, u32[]{:S(2)}) copy-start(pred[128]{0:T(512)(128)(4,1)} %constant.13.clone.1) | copy-start | bytes 388
  40.7 2.5 copy-start.1
  81.2 4.2 %copy-start.2 = (bf16[8,256,128]{2,1,0:T(8,128)(2,1)S(1)}, bf16[8,256,128]{2,1,0:T(8,128)(2,1)}, u32[]{:S(2)}) copy-start(bf16[8,256,128]{2,1,0:T(8,128)(2,1)} %shard_map.165) | copy-start | bytes 1572868
  88.9 19.4 %copy-start.8 = (bf16[2048]{0:T(1024)(128)(2,1)S(1)}, bf16[2048]{0:T(1024)(128)(2,1)}, u32[]{:S(2)}) copy-start(bf16[2048]{0:T(1024)(128)(2,1)} %param.27) | copy-start | bytes 12292
  88.9 19.4 %copy-start.3 = (bf16[64,2048]{1,0:T(8,128)(2,1)S(1)}, bf16[64,2048]{1,0:T(8,128)(2,1)}, u32[]{:S(2)}) copy-start(bf16[64,2048]{1,0:T(8,128)(2,1)} %param.17) | copy-start | bytes 786436
  88.9 19.7 %copy-start.9 = (bf16[2048]{0:T(1024)(128)(2,1)S(1)}, bf16[2048]{0:T(1024)(128)(2,1)}, u32[]{:S(2)}) copy-start(bf16[2048]{0:T(1024)(128)(2,1)} %param.28) | copy-start | bytes 12292
  88.9 28.7 %copy-start.6 = (s32[256,2]{0,1:T(2,128)S(1)}, s32[256,2]{0,1:T(2,128)}, u32[]{:S(2)}) copy-start(s32[256,2]{0,1:T(2,128)} %param.29) | copy-start | bytes 6148
  228.2 22.3 %copy-start.10 = (f32[256,2]{0,1:T(2,128)S(1)}, f32[256,2]{0,1:T(2,128)}, u32[]{:S(2)}) copy-start(f32[256,2]{0,1:T(2,128)} %param.30) | copy-start | bytes 6148

commit v2 on v1

--- a/solution.py
+++ b/solution.py
@@ -142,40 +142,157 @@
     return lambda ref, index: ref.at[pl.ds(pl.multiple_of(index * height, height), height), :]
 
 
-def attend_kernel(block, scale_ref, query_ref, key_ref, value_ref, row_ref, col_ref, out_ref):
-    scale = scale_ref[0]
-    total_rows = query_ref.shape[0]
+def greet(axes):
+    barrier = pltpu.get_barrier_semaphore()
+    for axis, count in axes:
+        me = lax.axis_index(axis)
+        for step in range(1, count):
+            pl.semaphore_signal(
+                barrier,
+                inc=1,
+                device_id={axis: lax.rem(me + step, count)},
+                device_id_type=pl.DeviceIdType.MESH,
+            )
+    pl.semaphore_wait(barrier, sum(count - 1 for _, count in axes))
+
+
+def send(source, target, sent, landed, axis, peer):
+    return pltpu.make_async_remote_copy(
+        src_ref=source,
+        dst_ref=target,
+        send_sem=sent,
+        recv_sem=landed,
+        device_id={axis: peer},
+        device_id_type=pl.DeviceIdType.MESH,
+    )
+
+
+def attend_block(block, index, width, starts, main, tail, gate_rows, mixed):
+    query_at, key_at, value_at = starts
+    scale = width ** (-0.5)
+    start = index * block
+    here = slice(start, start + block)
+    early = slice(0, start)
+    dims = (((1,), (1,)), ((), ()))
+
+    def values(rows):
+        if value_at is None:
+            return tail[rows, :]
+        return main[rows, value_at : value_at + width]
+
+    gate = jnp.broadcast_to(gate_rows[0:1, here], (128, block)).T[:, 0:1]
+    query = main[here, query_at : query_at + width]
     lower = lax.broadcasted_iota(jnp.int32, (block, block), 1) <= lax.broadcasted_iota(
         jnp.int32, (block, block), 0
     )
-    dims = (((1,), (1,)), ((), ()))
-    for start in range(0, total_rows, block):
-        here = slice(start, start + block)
-        query = query_ref[here, :]
-        gate = col_ref[here, :]
-        diag = lax.dot_general(query, key_ref[here, :], dims, preferred_element_type=jnp.float32)
-        diag = diag * scale + gate - row_ref[0:1, here]
-        diag = jnp.where(lower, diag, big_neg)
-        highest = jnp.max(diag, axis=1, keepdims=True)
-        if start:
-            early = slice(0, start)
-            score = lax.dot_general(
-                query, key_ref[early, :], dims, preferred_element_type=jnp.float32
+
+    def scores(rows):
+        dot = lax.dot_general(
+            query,
+            main[rows, key_at : key_at + width],
+            dims,
+            preferred_element_type=jnp.float32,
+        )
+        return dot * scale + gate - gate_rows[0:1, rows]
+
+    diag = jnp.where(lower, scores(here), big_neg)
+    highest = jnp.max(diag, axis=1, keepdims=True)
+    if start:
+        score = scores(early)
+        highest = jnp.maximum(highest, jnp.max(score, axis=1, keepdims=True))
+    expo = jnp.exp(diag - highest)
+    total = jnp.sum(expo, axis=1, keepdims=True)
+    result = jnp.dot(expo.astype(jnp.bfloat16), values(here), preferred_element_type=jnp.float32)
+    if start:
+        expo = jnp.exp(score - highest)
+        total = total + jnp.sum(expo, axis=1, keepdims=True)
+        result = result + jnp.dot(
+            expo.astype(jnp.bfloat16), values(early), preferred_element_type=jnp.float32
+        )
+    result = (result / total).astype(jnp.bfloat16)
+    if result.shape[1] < mixed.shape[1]:
+        fill = jnp.zeros((block, mixed.shape[1] - result.shape[1]), jnp.bfloat16)
+        result = jnp.concatenate([result, fill], axis=1)
+    mixed[here, :] = result
+
+
+def attend_kernel(
+    count, rows, width_a, width_b, packed, late, gates, back,
+    main, tail, gate_rows, mixed, sent, landed, own_sem, back_sent, back_landed,
+):
+    me = lax.axis_index("sp")
+    second = lax.rem(me, 2) == 1
+    greet([("sp", count)])
+
+    def rows_of(ref, index):
+        return ref.at[pl.ds(pl.multiple_of(index * rows, rows), rows), :]
+
+    def pieces(dest, sender):
+        return (
+            (packed.at[dest], rows_of(main, sender)),
+            (gates.at[dest], gate_rows.at[:, pl.ds(pl.multiple_of(sender * rows, rows), rows)]),
+            (late.at[dest // 2], rows_of(tail, sender)),
+        )
+
+    def remote(kind, step, dest, sender):
+        source, target = pieces(dest, sender)[kind]
+        return send(source, target, sent.at[kind, step], landed.at[kind, step], "sp", dest)
+
+    def own(kind):
+        source, target = pieces(me, me)[kind]
+        return pltpu.make_async_copy(source, target, own_sem.at[kind])
+
+    for step in range(1, count):
+        dest = lax.rem(me + step, count)
+        remote(0, step, dest, me).start()
+        remote(1, step, dest, me).start()
+        pl.when(lax.rem(dest, 2) == 1)(lambda: remote(2, step, dest, me).start())
+    own(0).start()
+    own(1).start()
+    pl.when(second)(lambda: own(2).start())
+    own(0).wait()
+    own(1).wait()
+    pl.when(second)(lambda: own(2).wait())
+
+    def back_copy(dest, sender):
+        return send(
+            rows_of(mixed, dest), back.at[sender], back_sent.at[dest], back_landed.at[sender],
+            "sp", dest,
+        )
+
+    def back_own():
+        return pltpu.make_async_copy(rows_of(mixed, me), back.at[me], back_sent.at[me])
+
+    for index in range(count):
+
+        @pl.when(me != index)
+        def _():
+            step = lax.rem(me - index + count, count)
+            remote(0, step, me, index).wait_recv()
+            remote(1, step, me, index).wait_recv()
+            pl.when(second)(lambda: remote(2, step, me, index).wait_recv())
+
+        @pl.when(second)
+        def _():
+            attend_block(rows, index, width_b, (0, width_b, None), main, tail, gate_rows, mixed)
+
+        @pl.when(jnp.logical_not(second))
+        def _():
+            attend_block(
+                rows, index, width_a, (0, width_a, 2 * width_a), main, tail, gate_rows, mixed
             )
-            score = score * scale + gate - row_ref[0:1, early]
-            highest = jnp.maximum(highest, jnp.max(score, axis=1, keepdims=True))
-        expo = jnp.exp(diag - highest)
-        total = jnp.sum(expo, axis=1, keepdims=True)
-        mixed = jnp.dot(
-            expo.astype(jnp.bfloat16), value_ref[here, :], preferred_element_type=jnp.float32
-        )
-        if start:
-            expo = jnp.exp(score - highest)
-            total = total + jnp.sum(expo, axis=1, keepdims=True)
-            mixed = mixed + jnp.dot(
-                expo.astype(jnp.bfloat16), value_ref[early, :], preferred_element_type=jnp.float32
-            )
-        out_ref[here, :] = (mixed / total).astype(jnp.bfloat16)
+
+        pl.when(me != index)(lambda: back_copy(index, me).start())
+        pl.when(me == index)(lambda: back_own().start())
+
+    for step in range(1, count):
+        dest = lax.rem(me + step, count)
+        remote(0, step, dest, me).wait_send()
+        remote(1, step, dest, me).wait_send()
+        pl.when(lax.rem(dest, 2) == 1)(lambda: remote(2, step, dest, me).wait_send())
+        back_copy(dest, me).wait_send()
+        back_copy(me, dest).wait_recv()
+    back_own().wait()
 
 
 def headwise_attention(
@@ -186,7 +303,6 @@
     width_a = query_a.shape[1] // heads
     width_b = query_b.shape[1] // heads
     count = lax.axis_size("sp")
-    me = lax.axis_index("sp")
 
     def split(values, width):
         return values.reshape(rows, heads, width).transpose(1, 0, 2)
@@ -196,48 +312,193 @@
         [split(query_a, width_a), split(key_a, width_a), split(value_a, width_a), pad], axis=2
     )
     second = jnp.concatenate([split(query_b, width_b), split(key_b, width_b)], axis=2)
-    packed = jnp.concatenate([first, second], axis=0)
+    packed = jnp.stack([first, second], axis=1).reshape(count, rows, 2 * width_b)
     late = split(value_b, width_b)
-    gates = cum_gates.transpose(1, 2, 0).reshape(2 * heads, 1, rows)
-    gates = jnp.broadcast_to(gates, (2 * heads, 8, rows))
-    main, tail, gate_rows = exchange(
-        [packed, late, gates],
-        [
-            (count * rows, 2 * width_b),
-            (count * rows, width_b),
-            (8, count * rows),
+    gates = cum_gates.transpose(2, 1, 0).reshape(count, 1, rows)
+    gates = jnp.broadcast_to(gates, (count, 8, rows))
+    back = pl.pallas_call(
+        functools.partial(attend_kernel, count, rows, width_a, width_b),
+        out_shape=jax.ShapeDtypeStruct((count, rows, width_b), jnp.bfloat16),
+        in_specs=[pl.BlockSpec(memory_space=pltpu.VMEM)] * 3,
+        out_specs=pl.BlockSpec(memory_space=pltpu.VMEM),
+        scratch_shapes=[
+            pltpu.VMEM((count * rows, 2 * width_b), jnp.bfloat16),
+            pltpu.VMEM((count * rows, width_b), jnp.bfloat16),
+            pltpu.VMEM((8, count * rows), jnp.float32),
+            pltpu.VMEM((count * rows, width_b), jnp.bfloat16),
+            pltpu.SemaphoreType.DMA((3, count)),
+            pltpu.SemaphoreType.DMA((3, count)),
+            pltpu.SemaphoreType.DMA((3,)),
+            pltpu.SemaphoreType.DMA((count,)),
+            pltpu.SemaphoreType.DMA((count,)),
         ],
-        [
-            (item, row_block(rows), 0),
-            (lambda ref, index: ref.at[jnp.maximum(index - heads, 0)], row_block(rows), heads),
-            (item, column_block(rows), 0),
+        compiler_params=pltpu.CompilerParams(collective_id=1, has_side_effects=True),
+    )(packed, late, gates)
+    attn_a = back[0::2, :, :width_a].transpose(1, 0, 2).reshape(rows, heads * width_a)
+    attn_b = back[1::2].transpose(1, 0, 2).reshape(rows, heads * width_b)
+    return attn_a, attn_b
+
+
+def experts_kernel(
+    count, narrow, parts, outgoing, w_gate, w_up, w_down, returned,
+    gate_buf, up_buf, down_buf, piece, partial, taken, summed,
+    weight_sem, out_sent, out_landed, own_sem, fan_sent, fan_landed,
+    sum_sent, sum_landed, ret_sent, ret_landed,
+):
+    me = lax.axis_index("sp")
+    mine = lax.axis_index("tp")
+    _, slots, columns = outgoing.shape
+    weights = [
+        pltpu.make_async_copy(source, target, weight_sem.at[k])
+        for k, (source, target) in enumerate(
+            ((w_gate, gate_buf), (w_up, up_buf), (w_down, down_buf))
+        )
+    ]
+    for copy in weights:
+        copy.start()
+    greet([("sp", count), ("tp", narrow)])
+
+    def cols(index):
+        return pl.ds(pl.multiple_of(index * columns, columns), columns)
+
+    def step_rows(step):
+        return pl.ds(pl.multiple_of(step * slots, slots), slots)
+
+    def dispatch(step):
+        peer = lax.rem(me + step, count)
+        return send(
+            outgoing.at[peer], piece.at[step_rows(step), cols(mine)],
+            out_sent.at[step], out_landed.at[step], "sp", peer,
+        )
+
+    def fan(step, hop, owner):
+        place = piece.at[step_rows(step), cols(owner)]
+        return send(
+            place, place, fan_sent.at[step, hop], fan_landed.at[step, hop],
+            "tp", lax.rem(mine + hop, narrow),
+        )
+
+    for step in range(1, count):
+        dispatch(step).start()
+    own = pltpu.make_async_copy(
+        outgoing.at[me], piece.at[step_rows(0), cols(mine)], own_sem.at[0]
+    )
+    own.start()
+    for step in range(count):
+        if step:
+            dispatch(step).wait_recv()
+        else:
+            own.wait()
+        for hop in range(1, narrow):
+            fan(step, hop, mine).start()
+
+    for copy in weights:
+        copy.wait()
+    steps = count // parts
+    height = steps * slots
+
+    def part_rows(part):
+        return pl.ds(pl.multiple_of(part * height, height), height)
+
+    def give(part, hop):
+        peer = lax.rem(mine + hop, narrow)
+        return send(
+            partial.at[part_rows(part), cols(peer)], taken.at[hop - 1, part_rows(part), :],
+            sum_sent.at[part, hop], sum_landed.at[part, hop], "tp", peer,
+        )
+
+    def compute(part, carry):
+        for inner in range(steps):
+            for hop in range(1, narrow):
+                fan(part * steps + inner, hop, lax.rem(mine + narrow - hop, narrow)).wait_recv()
+        rows = piece[part_rows(part), :]
+        gate = jnp.dot(rows, gate_buf[...], preferred_element_type=jnp.float32)
+        upward = jnp.dot(rows, up_buf[...], preferred_element_type=jnp.float32)
+        hidden = (gate / (1.0 + jnp.exp(-gate)) * upward).astype(jnp.bfloat16)
+        partial[part_rows(part), :] = jnp.dot(
+            hidden, down_buf[...], preferred_element_type=jnp.float32
+        ).astype(jnp.bfloat16)
+        for hop in range(1, narrow):
+            give(part, hop).start()
+        return carry
+
+    lax.fori_loop(0, parts, compute, 0)
+
+    def give_back(step):
+        peer = lax.rem(me + count - step, count)
+        return send(
+            summed.at[step_rows(step), :], returned.at[me],
+            ret_sent.at[step], ret_landed.at[step], "sp", peer,
+        )
+
+    def returned_here(step):
+        sender = lax.rem(me + step, count)
+        return send(
+            summed.at[step_rows(step), :], returned.at[sender],
+            ret_sent.at[step], ret_landed.at[step], "sp", sender,
+        )
+
+    own_back = pltpu.make_async_copy(
+        summed.at[step_rows(0), :], returned.at[me], own_sem.at[1]
+    )
+    for part in range(parts):
+        here = slice(part * height, (part + 1) * height)
+        total = partial[here, cols(mine)].astype(jnp.float32)
+        for hop in range(1, narrow):
+            give(part, hop).wait_recv()
+            total = total + taken[hop - 1, here, :].astype(jnp.float32)
+        summed[here, :] = total.astype(jnp.bfloat16)
+        for inner in range(steps):
+            step = part * steps + inner
+            if step:
+                give_back(step).start()
+            else:
+                own_back.start()
+    for step in range(1, count):
+        returned_here(step).wait_recv()
+        give_back(step).wait_send()
+        dispatch(step).wait_send()
+    own_back.wait()
+    for hop in range(1, narrow):
+        for step in range(count):
+            fan(step, hop, mine).wait_send()
+        for part in range(parts):
+            give(part, hop).wait_send()
+
+
+def run_experts(outgoing, w_gate, w_up, w_down, parts):
+    count, slots, columns = outgoing.shape
+    narrow = lax.axis_size("tp")
+    total = count * slots
+    vmem = pl.BlockSpec(memory_space=pltpu.VMEM)
+    hbm = pl.BlockSpec(memory_space=pl.ANY)
+    dma = pltpu.SemaphoreType.DMA
+    return pl.pallas_call(
+        functools.partial(experts_kernel, count, narrow, parts),
+        out_shape=jax.ShapeDtypeStruct(outgoing.shape, jnp.bfloat16),
+        in_specs=[vmem, hbm, hbm, hbm],
+        out_specs=vmem,
+        scratch_shapes=[
+            pltpu.VMEM(w_gate.shape, jnp.bfloat16),
+            pltpu.VMEM(w_up.shape, jnp.bfloat16),
+            pltpu.VMEM(w_down.shape, jnp.bfloat16),
+            pltpu.VMEM((total, columns * narrow), jnp.bfloat16),
+            pltpu.VMEM((total, columns * narrow), jnp.bfloat16),
+            pltpu.VMEM((narrow - 1, total, columns), jnp.bfloat16),
+            pltpu.VMEM((total, columns), jnp.bfloat16),
+            dma((3,)),
+            dma((count,)),
+            dma((count,)),
+            dma((2,)),
+            dma((count, narrow)),
+            dma((count, narrow)),
+            dma((parts, narrow)),
+            dma((parts, narrow)),
+            dma((count,)),
+            dma((count,)),
         ],
-        "sp",
-        1,
-    )
-    narrow_head = me < heads
-    fill = jnp.zeros((count * rows, width_b - width_a), jnp.bfloat16)
-
-    def widen(index):
-        return jnp.concatenate([main[:, index * width_a : (index + 1) * width_a], fill], axis=1)
-
-    query = jnp.where(narrow_head, widen(0), main[:, :width_b])
-    keys = jnp.where(narrow_head, widen(1), main[:, width_b:])
-    values = jnp.where(narrow_head, widen(2), tail)
-    scale = jnp.where(narrow_head, width_a ** (-0.5), width_b ** (-0.5)).astype(jnp.float32)
-    mixed = pl.pallas_call(
-        functools.partial(attend_kernel, rows),
-        out_shape=jax.ShapeDtypeStruct((count * rows, width_b), jnp.bfloat16),
-        in_specs=[pl.BlockSpec(memory_space=pltpu.SMEM)]
-        + [pl.BlockSpec(memory_space=pltpu.VMEM)] * 5,
-        out_specs=pl.BlockSpec(memory_space=pltpu.VMEM),
-    )(scale.reshape(1), query, keys, values, gate_rows, gate_rows[0].reshape(-1, 1))
-    (back,) = exchange(
-        [mixed], [(count, rows, width_b)], [(row_block(rows), item, 0)], "sp", 2
-    )
-    attn_a = back[:heads, :, :width_a].transpose(1, 0, 2).reshape(rows, heads * width_a)
-    attn_b = back[heads:].transpose(1, 0, 2).reshape(rows, heads * width_b)
-    return attn_a, attn_b
+        compiler_params=pltpu.CompilerParams(collective_id=5, has_side_effects=True),
+    )(outgoing, w_gate, w_up, w_down)
 
 
 def gathered_attention(
@@ -375,35 +636,38 @@
         placing, column_rows, (((0,), (0,)), ((), ())), preferred_element_type=jnp.float32
     ).astype(jnp.bfloat16)
     outgoing = outgoing.reshape(group_size, slots, columns)
-    (arrived,) = exchange(
-        [outgoing], [(group_size, slots, columns)], [(item, item, 0)], "sp", 5
-    )
-    (piece,) = exchange(
-        [arrived.reshape(-1, columns)],
-        [(group_size * slots, columns * narrow)],
-        [(whole_ref, column_block(columns), 0)],
-        "tp",
-        6,
-    )
-    gate = jnp.dot(piece, w_gate[0], preferred_element_type=jnp.float32)
-    upward = jnp.dot(piece, w_up[0], preferred_element_type=jnp.float32)
-    hidden = (jax.nn.silu(gate) * upward).astype(jnp.bfloat16)
-    down = jnp.dot(hidden, w_down[0], preferred_element_type=jnp.float32).astype(jnp.bfloat16)
-    (downs,) = exchange(
-        [down],
-        [(narrow, group_size * slots, columns)],
-        [(column_block(columns), item, 0)],
-        "tp",
-        7,
-    )
-    summed = jnp.sum(downs.astype(jnp.float32), axis=0).astype(jnp.bfloat16)
-    (returned,) = exchange(
-        [summed.reshape(group_size, slots, columns)],
-        [(group_size, slots, columns)],
-        [(item, item, 0)],
-        "sp",
-        8,
-    )
+    if slots % 16 == 0 and group_size % 4 == 0:
+        returned = run_experts(outgoing, w_gate[0], w_up[0], w_down[0], 4)
+    else:
+        (arrived,) = exchange(
+            [outgoing], [(group_size, slots, columns)], [(item, item, 0)], "sp", 10
+        )
+        (piece,) = exchange(
+            [arrived.reshape(-1, columns)],
+            [(group_size * slots, columns * narrow)],
+            [(whole_ref, column_block(columns), 0)],
+            "tp",
+            6,
+        )
+        gate = jnp.dot(piece, w_gate[0], preferred_element_type=jnp.float32)
+        upward = jnp.dot(piece, w_up[0], preferred_element_type=jnp.float32)
+        hidden = (jax.nn.silu(gate) * upward).astype(jnp.bfloat16)
+        down = jnp.dot(hidden, w_down[0], preferred_element_type=jnp.float32).astype(jnp.bfloat16)
+        (downs,) = exchange(
+            [down],
+            [(narrow, group_size * slots, columns)],
+            [(column_block(columns), item, 0)],
+            "tp",
+            7,
+        )
+        summed = jnp.sum(downs.astype(jnp.float32), axis=0).astype(jnp.bfloat16)
+        (returned,) = exchange(
+            [summed.reshape(group_size, slots, columns)],
+            [(group_size, slots, columns)],
+            [(item, item, 0)],
+            "sp",
+            8,
+        )
     mixture_cols = jnp.dot(
         weighting,
         returned.reshape(group_size * slots, columns).astype(jnp.float32),

time: 266 us -> 181 us (0.68)
  Pallas kernels: 207 us -> 154 us
  matrix products: 30.9 us -> 11.3 us
  other arithmetic: 12.2 us -> 5.13 us
    pallas_call x9 -> x3, Pallas kernels: 200 us -> 33.2 us  [exchange(): pl.pallas_call(functools.partial(exchange_kernel, axis, count, plans), ou...]
    pallas_call x1 -> x2, Pallas kernels: 7.63 us -> 120 us  [the longest x1 76 us: run_experts(): pl.pallas_call(functools.partial(experts_kernel, count, narrow, parts), o...]
    dot_general x2 -> x0, matrix products: 19.7 us -> none  [the longest x1 12.3 us: per_device(): jnp.dot(hidden, w_down[0], preferred_element_type=jnp.float32)]
    reduce_sum x1 -> x0, other arithmetic: 3.18 us -> none  [per_device(): summed = jnp.sum(downs.astype(jnp.float32), axis=0).astype(jnp.bfloat16)]
    select_n x1 -> x0, other arithmetic: 2.7 us -> none  [headwise_attention(): keys = jnp.where(narrow_head, widen(1), main[:, width_b:])]
    unnamed x30 -> x22, local copies, waits for them, and re-layouts: 4.66 us -> 6.44 us
where the time goes in v2:
time: 181 us
  Pallas kernels  154 us (85%)
  matrix products  11.3 us (6%)
  local copies, waits for them, and re-layouts  10.7 us (6%)
  other arithmetic  5.13 us (3%)
    pallas_call x1, Pallas kernels, run_experts(): pl.pallas_call(functools.partial(experts_kernel, count, narrow, parts), o...  76 us
    pallas_call x1, Pallas kernels, headwise_attention(): pl.pallas_call(functools.partial(attend_kernel, count, rows, width_a, wid...  44.5 us
    pallas_call x3, Pallas kernels, exchange(): pl.pallas_call(functools.partial(exchange_kernel, axis, count, plans), ou...  33.2 us
    unnamed x22, local copies, waits for them, and re-layouts  6.44 us

profile of v2, /device:TPU:0, one launch (start us, length us, event | category | flops | bytes accessed | tf_op | source)
XLA Modules:
  0.0 180.9 jit_solution(17339406331652838396)
XLA Ops:
  0.0 0.0 copy-start
  0.0 1.2 copy.46
  1.2 1.1 copy.45
  2.3 1.0 copy.42
  3.3 1.0 copy.43
  4.4 1.0 copy.44
  5.4 0.1 pad.7.clone
  5.5 0.1 maximum_bitcast_fusion
  5.6 0.1 pad_maximum_fusion
  5.7 0.0 copy-start.4
  5.7 1.3 copy.47
  7.1 1.1 copy.48
  8.1 0.8 copy.49
  9.0 0.0 copy-done.4
  9.0 0.6 broadcast_in_dim.48.gates
  9.6 44.5 %shard_map.163 = bf16[8,256,128]{2,1,0:T(8,128)(2,1)} custom-call(bf16[8,256,256]{2,1,0:T(8,128)(2,1)} %bitcast.46, bf16[4,256,128]{2,1,0:T(8,128)(2,1)} %bitcast.52, f32[8,8,256]{2,1,0:T(8,128)} %broadcast_in_dim.48.gates), custom_call_target="tpu_custom_call" | custom-call | tf_op jit(solution)/shard_map/pallas_call | solution.py:319
  54.1 0.0 copy-start.1
  54.1 1.0 slice_bitcast_fusion.1
  55.2 0.1 copy.51
  55.3 3.0 %fusion.12 = f32[256,2048]{1,0:T(8,128)} fusion(bf16[256,256]{0,1:T(8,128)(2,1)S(1)} %bitcast.54, bf16[256,2048]{1,0:T(8,128)(2,1)} %param.25), kind=kOutput, calls=%fused_computation.33 | convolution fusion | flops 268435456 | bytes 3276800 | tf_op jit(solution)/shard_map/dot_general | solution.py:599
  58.3 0.0 copy-done.1
  58.3 0.1 copy.52
  58.5 0.0 copy-done
  58.5 3.3 %fusion.refs_0_ = bf16[256,2048]{1,0:T(8,128)(2,1)} fusion(f32[256,2048]{1,0:T(8,128)} %fusion.12, bf16[256,512]{0,1:T(8,128)(2,1)S(1)} %bitcast.53, bf16[512,2048]{1,0:T(8,128)(2,1)S(1)} %copy-done), kind=kOutput, calls=%fused_computation.1 | convolution fusion | flops 537919488 | bytes 5505024 | tf_op jit(solution)/shard_map/dot_general | solution.py:600
  61.8 0.0 copy-start.5
  61.8 0.0 copy-start.2
  61.8 0.0 copy-start.6
  61.8 18.1 %shard_map.164 = bf16[4,64,2048]{2,1,0:T(8,128)(2,1)} custom-call(bf16[256,2048]{1,0:T(8,128)(2,1)} %fusion.refs_0_), custom_call_target="tpu_custom_call" | custom-call | tf_op jit(solution)/shard_map/pallas_call | solution.py:112
  79.9 0.0 copy-start.3
  79.9 1.4 reduce_sum.48
  81.3 0.2 fusion.2
  81.5 0.0 copy-done.5
  81.5 0.0 copy-done.2
  81.5 0.3 fusion.6
  81.8 0.0 copy-done.6
  81.8 0.8 fusion.8.refs_0_
  82.7 8.2 %shard_map.165 = bf16[256,512]{1,0:T(8,128)(2,1)} custom-call(bf16[64,2048]{1,0:T(8,128)(2,1)} %fusion.8.refs_0_), custom_call_target="tpu_custom_call" | custom-call | tf_op jit(solution)/shard_map/pallas_call | solution.py:112
  90.9 0.0 copy-done.3
  90.9 0.2 convolution_convert_fusion.2
  91.1 0.2 fusion.1
  91.3 2.2 %convolution_convert_fusion = bf16[640,512]{1,0:T(8,128)(2,1)} fusion(pred[256,640]{1,0:T(8,128)(4,1)S(1)} %fusion.1, bf16[256,512]{1,0:T(8,128)(2,1)} %shard_map.165), kind=kOutput, calls=%fused_computation.2 | convolution fusion | flops 168099840 | bytes 1081344 | tf_op jit(solution)/shard_map/dot_general | solution.py:635
  93.5 0.0 copy-start.7
  93.5 76.0 %shard_map.166 = bf16[8,80,512]{2,1,0:T(8,128)(2,1)} custom-call(bf16[8,80,512]{2,1,0:T(8,128)(2,1)} %bitcast.48, bf16[2048,1024]{1,0:T(8,128)(2,1)} %bitcast.43, bf16[2048,1024]{1,0:T(8,128)(2,1)} %bitcast.44, bf16[1024,2048]{1,0:T(8,128)(2,1)} %bitcast.45), custom_call_target="tpu_custom_call" | custom-call | tf_op jit(solution)/shard_map/pallas_call | solution.py:476
  169.4 0.0 copy-done.7
  169.5 0.2 select_reduce_fusion
  169.7 2.6 %convolution_convert_fusion.1.refs_0_ = bf16[256,512]{1,0:T(8,128)(2,1)} fusion(f32[256,640]{1,0:T(8,128)S(1)} %select_reduce_fusion, bf16[640,512]{1,0:T(8,128)(2,1)} %bitcast.47), kind=kOutput, calls=%fused_computation.6 | convolution fusion | flops 1006764032 | bytes 1572864 | tf_op jit(solution)/shard_map/dot_general | solution.py:671
  172.3 6.9 %shard_map.167 = bf16[64,2048]{1,0:T(8,128)(2,1)} custom-call(bf16[256,512]{1,0:T(8,128)(2,1)} %convolution_convert_fusion.1.refs_0_), custom_call_target="tpu_custom_call" | custom-call | tf_op jit(solution)/shard_map/pallas_call | solution.py:112
  179.2 1.7 fusion.9
  (11 shorter events, 0.1 us)
Async XLA Ops:
  0.0 58.5 %copy-start = (bf16[512,2048]{1,0:T(8,128)(2,1)S(1)}, bf16[512,2048]{1,0:T(8,128)(2,1)}, u32[]{:S(2)}) copy-start(bf16[512,2048]{1,0:T(8,128)(2,1)} %param.26) | copy-start | bytes 6291460
  5.7 3.3 %copy-start.4 = (f32[256,2,4]{0,2,1:T(4,128)S(1)}, f32[256,2,4]{0,2,1:T(4,128)}, u32[]{:S(2)}) copy-start(f32[256,2,4]{0,2,1:T(4,128)} %param.24) | copy-start | bytes 24580
  54.1 4.2 %copy-start.1 = (bf16[8,256,128]{2,1,0:T(8,128)(2,1)S(1)}, bf16[8,256,128]{2,1,0:T(8,128)(2,1)}, u32[]{:S(2)}) copy-start(bf16[8,256,128]{2,1,0:T(8,128)(2,1)} %shard_map.163) | copy-start | bytes 1572868
  61.8 19.7 %copy-start.5 = (bf16[2048]{0:T(1024)(128)(2,1)S(1)}, bf16[2048]{0:T(1024)(128)(2,1)}, u32[]{:S(2)}) copy-start(bf16[2048]{0:T(1024)(128)(2,1)} %param.27) | copy-start | bytes 12292
  61.8 19.7 %copy-start.2 = (bf16[64,2048]{1,0:T(8,128)(2,1)S(1)}, bf16[64,2048]{1,0:T(8,128)(2,1)}, u32[]{:S(2)}) copy-start(bf16[64,2048]{1,0:T(8,128)(2,1)} %param.17) | copy-start | bytes 786436
  61.8 20.0 %copy-start.6 = (bf16[2048]{0:T(1024)(128)(2,1)S(1)}, bf16[2048]{0:T(1024)(128)(2,1)}, u32[]{:S(2)}) copy-start(bf16[2048]{0:T(1024)(128)(2,1)} %param.28) | copy-start | bytes 12292
  79.9 11.0 %copy-start.3 = (s32[256,2]{0,1:T(2,128)S(1)}, s32[256,2]{0,1:T(2,128)}, u32[]{:S(2)}) copy-start(s32[256,2]{0,1:T(2,128)} %param.29) | copy-start | bytes 6148
  93.5 76.0 %copy-start.7 = (f32[256,2]{0,1:T(2,128)S(1)}, f32[256,2]{0,1:T(2,128)}, u32[]{:S(2)}) copy-start(f32[256,2]{0,1:T(2,128)} %param.30) | copy-start | bytes 6148
